TPU v7x, 32 devices: a whole 2x2x4 slice. The times are simulated.
32 devices in a mesh: ep: 8 (over z, x), tp: 4 (over y, core).
Axes of the slice: x: 2, y: 2, z: 4, core: 2. Of those that a mesh axis runs over, the one named last changes fastest.
Arguments:
- queries: bfloat16 [4096, 2048], P('ep', 'tp'), may hold values from -5 to 5
- key_rows: bfloat16 [4096, 2048], P('ep', 'tp'), may hold values from -5 to 5
- values: bfloat16 [4096, 2048], P('ep', 'tp'), may hold values from -6 to 6
- forget_log: float32 [4096, 16], P(None, 'tp'), may hold values from -515 to 0, as said below
- out_weight: bfloat16 [2048, 4096], P(None, 'tp'), may hold values from -1 to 1
- expert_input: bfloat16 [1024, 4096], P(('ep', 'tp')), may hold values from -6 to 6
- norm_gain: float32 [4096], replicated, may hold values from 0.1 to 1.9
- route_ids: int32 [1024, 2], P('ep'), may hold values from 0 to 7, all different within a row; in each aligned block of 128 rows (0 to 127, 128 to 255, ...) at most 64 rows name the same one
- route_weights: float32 [1024, 2], P('ep'), may hold values from 0.2 to 1
- gate_weight: bfloat16 [8, 4096, 2048], P('ep', None, 'tp'), may hold values from -0.09375 to 0.09375
- up_weight: bfloat16 [8, 4096, 2048], P('ep', None, 'tp'), may hold values from -0.09375 to 0.09375
- down_weight: bfloat16 [8, 2048, 4096], P('ep', None, 'tp'), may hold values from -0.125 to 0.125
Outputs:
- mixer_out: bfloat16 [4096, 4096], P('ep', 'tp')
- expert_out: bfloat16 [1024, 4096], P('ep', 'tp')
Inputs may be any that keep to these rules, and one draw needn't show every extreme that they name: forget_log[t, h] is the sum of the log forget gates of head h at positions 0 to t of the one sequence; it never rises along positions. `route_ids`: each row names 2 different experts. In each aligned block of 128 rows (the rows of one index of ep) no expert is named by more than 64 rows, and some block reaches 64.
All inputs are finite; a program needn't handle non-finite values.
Results may differ from a plain program's by a relative error of at most 0.0071.
Values may be sent and summed in bfloat16 or wider, within the bound.
A program may use at most 64 MiB of HBM per device.

v0:
```python
import functools
import math

import jax
import jax.numpy as jnp
from jax import lax
from jax.experimental import pallas as pl
from jax.experimental.pallas import tpu as pltpu
from jax.sharding import PartitionSpec as P

EPSILON = 1e-05
LOG2E = math.log2(math.e)


def attention_kernel(
    n, tp, heads, gate_row, gate_col, q_ref, k_ref, v_ref, pick_ref, token_ref,
    out_ref, routed_ref,
    k_buf, v_buf, q_buf, o_buf, token_buf, leave_buf,
    recv_k, recv_v, recv_q, recv_o, send_k, send_v, send_q, send_o, pass_k, pass_v,
    send_t, recv_t, send_a, recv_a, send_f, recv_f,
):
    members = n // heads
    rows = k_ref.shape[0]
    width = k_ref.shape[1] // heads
    chunk = rows // members
    me = lax.axis_index("ep")
    my_member = me % members
    my_head = me // members
    my_tp = lax.axis_index("tp")
    tokens = token_ref.shape[0]

    barrier = pltpu.get_barrier_semaphore()

    @pl.loop(1, n)
    def _(step):
        pl.semaphore_signal(barrier, inc=1, device_id={"ep": (me + step) % n})

    @pl.loop(1, tp)
    def _(step):
        pl.semaphore_signal(barrier, inc=1, device_id={"tp": (my_tp + step) % tp})

    pl.semaphore_wait(barrier, n + tp - 2)

    def k_copy(target, head):
        cols = pl.ds(pl.multiple_of(head * width, width), width)
        return pltpu.make_async_remote_copy(
            src_ref=k_ref.at[:, cols], dst_ref=k_buf.at[me], send_sem=send_k.at[head],
            recv_sem=recv_k.at[me], device_id={"ep": target},
        )

    def v_copy(target, head):
        cols = pl.ds(pl.multiple_of(head * width, width), width)
        return pltpu.make_async_remote_copy(
            src_ref=v_ref.at[:, cols], dst_ref=v_buf.at[me], send_sem=send_v.at[head],
            recv_sem=recv_v.at[me], device_id={"ep": target},
        )

    def q_copy(target):
        cols = pl.ds(pl.multiple_of((target // members) * width, width), width)
        part = pl.ds(pl.multiple_of((target % members) * chunk, chunk), chunk)
        return pltpu.make_async_remote_copy(
            src_ref=q_ref.at[part, cols], dst_ref=q_buf.at[me], send_sem=send_q.at[target],
            recv_sem=recv_q.at[me], device_id={"ep": target},
        )

    def pass_copies(source, target):
        return (
            pltpu.make_async_remote_copy(
                src_ref=k_buf.at[source], dst_ref=k_buf.at[source],
                send_sem=pass_k.at[source, target % members],
                recv_sem=recv_k.at[source], device_id={"ep": target},
            ),
            pltpu.make_async_remote_copy(
                src_ref=v_buf.at[source], dst_ref=v_buf.at[source],
                send_sem=pass_v.at[source, target % members],
                recv_sem=recv_v.at[source], device_id={"ep": target},
            ),
        )

    def back_copy(source):
        cols = pl.ds(pl.multiple_of(my_head * width, width), width)
        part = pl.ds(pl.multiple_of(my_member * chunk, chunk), chunk)
        return pltpu.make_async_remote_copy(
            src_ref=o_buf.at[source], dst_ref=out_ref.at[part, cols], send_sem=send_o.at[source],
            recv_sem=recv_o.at[me], device_id={"ep": source},
        )

    def token_spot(owner):
        return token_buf.at[pl.ds(pl.multiple_of(owner * tokens, tokens), tokens), :]

    def token_copy(target):
        return pltpu.make_async_remote_copy(
            src_ref=token_ref, dst_ref=token_spot(my_tp), send_sem=send_t.at[target],
            recv_sem=recv_t.at[my_tp], device_id={"tp": target},
        )

    def leave_copy(target):
        return pltpu.make_async_remote_copy(
            src_ref=leave_buf.at[target], dst_ref=routed_ref.at[me, my_tp],
            send_sem=send_a.at[target], recv_sem=recv_a.at[me], device_id={"ep": target},
        )

    def spread_copy(source, target):
        spot = routed_ref.at[source, my_tp]
        return pltpu.make_async_remote_copy(
            src_ref=spot, dst_ref=spot, send_sem=send_f.at[source, target],
            recv_sem=recv_f.at[source, my_tp], device_id={"tp": target},
        )

    pltpu.make_async_copy(token_ref, token_spot(my_tp), recv_t.at[my_tp]).start()

    @pl.loop(1, tp)
    def _(step):
        token_copy((my_tp + step) % tp).start()

    own_cols = pl.ds(pl.multiple_of(my_head * width, width), width)
    own_part = pl.ds(pl.multiple_of(my_member * chunk, chunk), chunk)
    pltpu.make_async_copy(k_ref.at[:, own_cols], k_buf.at[me], recv_k.at[me]).start()
    pltpu.make_async_copy(v_ref.at[:, own_cols], v_buf.at[me], recv_v.at[me]).start()
    pltpu.make_async_copy(q_ref.at[own_part, own_cols], q_buf.at[me], recv_q.at[me]).start()

    @pl.loop(1, heads)
    def _(step):
        head = (my_head + step) % heads
        k_copy(head * members + my_member, head).start()
        v_copy(head * members + my_member, head).start()

    @pl.loop(1, n)
    def _(step):
        q_copy((me + step) % n).start()

    @pl.loop(0, tp)
    def _(owner):
        pltpu.make_async_copy(token_spot(owner), token_spot(owner), recv_t.at[owner]).wait()

    @pl.loop(0, n)
    def _(target):
        leave_buf[target] = jnp.dot(
            pick_ref[target], token_buf[...], preferred_element_type=jnp.float32
        ).astype(leave_buf.dtype)

    pltpu.make_async_copy(leave_buf.at[me], routed_ref.at[me, my_tp], recv_a.at[me]).start()

    @pl.loop(1, n)
    def _(step):
        leave_copy((me + step) % n).start()

    def landed(source):
        pltpu.make_async_copy(k_buf.at[source], k_buf.at[source], recv_k.at[source]).wait()
        pltpu.make_async_copy(v_buf.at[source], v_buf.at[source], recv_v.at[source]).wait()

    @pl.loop(0, heads)
    def _(step):
        source = ((my_head + step) % heads) * members + my_member
        landed(source)

        @pl.loop(1, members)
        def _(other):
            for copy in pass_copies(source, my_head * members + (my_member + other) % members):
                copy.start()

    column = lax.broadcasted_iota(jnp.int32, (chunk, rows), 1)
    line = lax.broadcasted_iota(jnp.int32, (chunk, rows), 0) + my_member * chunk
    causal = column <= line
    factor = LOG2E * width ** (-0.5)

    @pl.loop(0, n)
    def _(i):
        pltpu.make_async_copy(q_buf.at[i], q_buf.at[i], recv_q.at[i]).wait()

        @pl.when(i % members != my_member)
        def _():
            landed(i)

        query = q_buf[i]
        line_gate = gate_col[i]

        def scores_of(j):
            raw = lax.dot_general(
                query, k_buf[j], (((1,), (1,)), ((), ())), preferred_element_type=jnp.float32
            )
            return raw * factor + (line_gate - gate_row[j])

        def weigh(weights, j):
            return jnp.dot(
                weights.astype(jnp.bfloat16), v_buf[j], preferred_element_type=jnp.float32
            )

        scores = jnp.where(causal, scores_of(i), -jnp.inf)
        top = jnp.max(scores, axis=1, keepdims=True)
        weights = jnp.exp2(scores - top)
        total = jnp.sum(weights, axis=1, keepdims=True)
        held = weigh(weights, i)

        def fold(j, state):
            top, total, held = state
            scores = scores_of(j)
            newest = jnp.maximum(top, jnp.max(scores, axis=1, keepdims=True))
            shrink = jnp.exp2(top - newest)
            weights = jnp.exp2(scores - newest)
            total = total * shrink + jnp.sum(weights, axis=1, keepdims=True)
            held = held * shrink + weigh(weights, j)
            return newest, total, held

        top, total, held = lax.fori_loop(0, i, fold, (top, total, held))
        o_buf[i] = (held / total).astype(o_buf.dtype)

        @pl.when(i != me)
        def _():
            back_copy(i).start()

        source = (me + n - i) % n
        spot = routed_ref.at[source, my_tp]
        pltpu.make_async_copy(spot, spot, recv_a.at[source]).wait()

        @pl.loop(1, tp)
        def _(step):
            spread_copy(source, (my_tp + step) % tp).start()

    own = pltpu.make_async_copy(o_buf.at[me], out_ref.at[own_part, own_cols], recv_o.at[me])
    own.start()

    @pl.loop(1, heads)
    def _(step):
        head = (my_head + step) % heads
        k_copy(head * members + my_member, head).wait_send()
        v_copy(head * members + my_member, head).wait_send()

    @pl.loop(1, n)
    def _(step):
        q_copy((me + step) % n).wait_send()
        back_copy((me + step) % n).wait_send()
        leave_copy((me + step) % n).wait_send()

    @pl.loop(1, tp)
    def _(step):
        token_copy((my_tp + step) % tp).wait_send()

    @pl.loop(0, n)
    def _(source):
        @pl.loop(1, tp)
        def _(step):
            other = (my_tp + step) % tp
            spread_copy(source, other).wait_send()
            spot = routed_ref.at[source, other]
            pltpu.make_async_copy(spot, spot, recv_f.at[source, other]).wait()

    @pl.loop(0, heads)
    def _(step):
        source = step * members + my_member

        @pl.loop(1, members)
        def _(other):
            for copy in pass_copies(source, my_head * members + (my_member + other) % members):
                copy.wait_send()

    @pl.loop(0, n)
    def _(i):
        cols = pl.ds(pl.multiple_of((i // members) * width, width), width)
        part = pl.ds(pl.multiple_of((i % members) * chunk, chunk), chunk)
        spot = out_ref.at[part, cols]
        pltpu.make_async_copy(spot, spot, recv_o.at[i]).wait()


def attention(queries, key_rows, values, forget_log, picks, normed):
    n, tp = lax.axis_size("ep"), lax.axis_size("tp")
    share, depth = picks.shape[1], normed.shape[1]
    rows, heads = queries.shape[0], forget_log.shape[1]
    width = queries.shape[1] // heads
    members = n // heads
    chunk = rows // members
    me = lax.axis_index("ep")
    gates = lax.dynamic_slice_in_dim(forget_log.T * LOG2E, me // members, 1, 0)
    gate_row = gates.reshape(n, 1, rows)
    gate_col = lax.dynamic_slice_in_dim(
        gates.reshape(n, members, chunk), me % members, 1, 1
    ).reshape(n, chunk, 1)
    vmem = pl.BlockSpec(memory_space=pltpu.VMEM)
    dma = pltpu.SemaphoreType.DMA
    blocks = n * (n + 1) // 2
    return pl.pallas_call(
        functools.partial(attention_kernel, n, tp, heads),
        out_shape=(
            jax.ShapeDtypeStruct((rows, heads * width), jnp.bfloat16),
            jax.ShapeDtypeStruct((n, tp, share, depth), jnp.bfloat16),
        ),
        in_specs=[vmem] * 7,
        out_specs=(vmem, vmem),
        scratch_shapes=[
            pltpu.VMEM((n, rows, width), jnp.bfloat16),
            pltpu.VMEM((n, rows, width), jnp.bfloat16),
            pltpu.VMEM((n, chunk, width), jnp.bfloat16),
            pltpu.VMEM((n, chunk, width), jnp.bfloat16),
            pltpu.VMEM((tp * normed.shape[0], depth), jnp.bfloat16),
            pltpu.VMEM((n, share, depth), jnp.bfloat16),
            dma((n,)), dma((n,)), dma((n,)), dma((n,)),
            dma((heads,)), dma((heads,)), dma((n,)), dma((n,)),
            dma((n, members)), dma((n, members)),
            dma((tp,)), dma((tp,)), dma((n,)), dma((n,)), dma((n, tp)), dma((n, tp)),
        ],
        compiler_params=pltpu.CompilerParams(
            collective_id=0, has_side_effects=True, vmem_limit_bytes=40 * 1024 * 1024
        ),
        cost_estimate=pl.CostEstimate(
            flops=40 * blocks * chunk * rows * width, bytes_accessed=8 * rows * heads * width,
            transcendentals=blocks * chunk * rows,
        ),
    )(gate_row, gate_col, queries, key_rows, values, picks, normed)


def slot_places(route_rows, experts, capacity):
    entries = route_rows.reshape(-1)
    matches = (entries[:, None] == jnp.arange(experts, dtype=jnp.int32)[None, :]).astype(jnp.int32)
    earlier = jnp.cumsum(matches, axis=0) - matches
    ranking = jnp.sum(earlier * matches, axis=1)
    return entries * capacity + ranking


def body(
    queries,
    key_rows,
    values,
    forget_log,
    out_weight,
    expert_input,
    norm_gain,
    route_ids,
    route_weights,
    gate_weight,
    up_weight,
    down_weight,
):
    as_float = expert_input.astype(jnp.float32)
    center = jnp.mean(as_float, axis=1, keepdims=True)
    variance = jnp.mean(jnp.square(as_float - center), axis=1, keepdims=True)
    normed = ((as_float - center) * lax.rsqrt(variance + EPSILON) * norm_gain).astype(jnp.bfloat16)
    block_rows = route_ids.shape[0]
    chosen = route_ids.shape[1]
    expert_local = gate_weight.shape[0]
    ep_count = lax.axis_size("ep")
    tp_count = lax.axis_size("tp")
    experts = expert_local * ep_count
    capacity = block_rows * chosen * 2 // experts
    places = slot_places(route_ids, experts, capacity)
    share_size = capacity // tp_count
    own_slots = lax.axis_index("tp") * share_size + jnp.arange(share_size, dtype=jnp.int32)
    part_slots = jnp.arange(experts, dtype=jnp.int32)[:, None] * capacity + own_slots[None, :]
    picks = jnp.any(
        part_slots.reshape(ep_count, expert_local * share_size)[:, :, None, None]
        == places.reshape(block_rows, chosen).T[None, None, :, :],
        axis=2,
    ).astype(jnp.bfloat16)
    attended, routed = attention(queries, key_rows, values, forget_log, picks, normed)
    arrived_rows = (
        routed.reshape(ep_count, tp_count, expert_local, share_size, routed.shape[3])
        .transpose(0, 2, 1, 3, 4)
        .reshape(ep_count, expert_local, capacity, routed.shape[3])
    )
    gate_part = jnp.einsum(
        "sxcd,xdf->sxcf", arrived_rows, gate_weight, preferred_element_type=jnp.float32
    )
    up_part = jnp.einsum(
        "sxcd,xdf->sxcf", arrived_rows, up_weight, preferred_element_type=jnp.float32
    )
    hidden = (jax.nn.silu(gate_part) * up_part).astype(jnp.bfloat16)
    slots_all = ep_count * expert_local * capacity
    flat_hidden = hidden.reshape(slots_all, hidden.shape[3])
    out_width = out_weight.shape[1]
    mixer_sum = jnp.dot(
        lax.all_gather(attended, "tp", axis=1, tiled=True),
        out_weight,
        preferred_element_type=jnp.float32,
    )
    part_rows = lax.all_gather(flat_hidden, "tp", axis=1, tiled=True)
    shaped = part_rows.reshape(ep_count, expert_local, capacity, part_rows.shape[1])
    product = jnp.einsum("sxcf,xfd->sxcd", shaped, down_weight, preferred_element_type=jnp.float32)
    expert_sum = product.reshape(slots_all, out_width)
    leaving = expert_sum.astype(jnp.bfloat16).reshape(ep_count, expert_local, capacity, out_width)
    returned = lax.all_to_all(leaving, "ep", split_axis=0, concat_axis=0, tiled=True)
    picked = jnp.take(returned.reshape(experts * capacity, out_width), places, axis=0).astype(
        jnp.float32
    )
    combined = jnp.sum(
        (picked * route_weights.reshape(-1)[:, None]).reshape(block_rows, chosen, out_width), axis=1
    )
    return (mixer_sum.astype(jnp.bfloat16), combined.astype(jnp.bfloat16))


def solution(mesh):
    placed = (
        P("ep", "tp"),
        P("ep", "tp"),
        P("ep", "tp"),
        P(None, "tp"),
        P(None, "tp"),
        P(("ep", "tp"), None),
        P(),
        P("ep", None),
        P("ep", None),
        P("ep", None, "tp"),
        P("ep", None, "tp"),
        P("ep", None, "tp"),
    )
    return jax.shard_map(
        body, mesh=mesh, in_specs=placed, out_specs=(P("ep", "tp"), P("ep", "tp")), check_vma=False
    )
```

profile of v0, /device:TPU:27, one launch (start us, length us, event | category | flops | bytes accessed | tf_op | source)
XLA Modules:
  0.0 210.9 jit_solution(14300768749676686987)
XLA Ops:
  7.2 0.8 copy.36
  8.3 0.5 broadcast.137
  8.8 1.5 fusion.32
  10.4 0.3 reshape.188.gate_col
  10.8 0.6 reduce-window.6
  11.9 0.7 broadcast_multiply_fusion
  12.8 1.1 convert_reduce_fusion
  13.9 1.2 fusion.26
  15.1 1.1 fusion.28.token_ref
  16.3 1.0 copy-done
  17.3 1.0 copy-done.1
  18.3 1.0 copy-done.2
  19.4 90.3 %shard_map.131 = (bf16[512,512]{1,0:T(8,128)(2,1)}, bf16[8,4,16,4096]{3,2,1,0:T(8,128)(2,1)S(1)}) custom-call(f32[8,1,512]{2,1,0:T(1,128)S(1)} %bitcast.71, f32[8,256,1]{2,1,0:T(8,128)S(1)} %reshape.188.gate_col, bf16[512,512]{1,0:T(8,128)(2,1)S(1)} %copy-done, bf16[512,512]{1,0:T(8,128)(2,1)S(1)} %copy-done.1, bf16[512,512]{1,0:T(8,128)(2,1)S(1)} %copy-done.2, ...), custom_call_target="tpu_custom_call" | custom-call | flops 24159191040 | bytes 2097152 | tf_op jit(solution)/shard_map/pallas_call | solution.py:281
  109.7 2.3 %fusion.12 = f32[8,1,64,512]{3,2,0,1:T(8,128)S(1)} fusion(bf16[8,64,4096]{2,1,0:T(8,128)(2,1)S(1)} %bitcast.72, bf16[1,4096,512]{2,1,0:T(8,128)(2,1)S(1)} %copy-done.5), kind=kOutput, calls=%fused_computation.10 | convolution fusion | flops 2147483648 | bytes 9437184 | tf_op jit(solution)/shard_map/sxcd,xdf->sxcf/dot_general | solution.py:359
  112.1 3.2 %fusion.21 = bf16[8,1,64,512]{3,2,0,1:T(8,128)(2,1)} fusion(bf16[8,64,4096]{2,1,0:T(8,128)(2,1)S(1)} %bitcast.73, bf16[1,4096,512]{2,1,0:T(8,128)(2,1)S(1)} %copy-done.6, f32[8,1,64,512]{3,2,0,1:T(8,128)S(1)} %fusion.12), kind=kOutput, calls=%fused_computation.13 | convolution fusion | flops 2149056512 | bytes 9961472 | tf_op jit(solution)/shard_map/sxcd,xdf->sxcf/dot_general | solution.py:362
  115.3 0.7 all-gather.3.cloned.1.call-update
  116.0 48.6 %all-gather.5.cloned.1.call-done = bf16[512,2048]{1,0:T(8,128)(2,1)} async-done(((bf16[512,512]{1,0:T(8,128)(2,1)}), bf16[512,2048]{1,0:T(8,128)(2,1)}) %all-gather.5.cloned.1.call-update) | async-done | bytes 2097168 | tf_op jit(solution)/shard_map/all_gather | solution.py:374
  164.6 6.2 %fusion.9 = bf16[8,1,64,1024]{3,2,1,0:T(8,128)(2,1)} fusion(bf16[8,64,2048]{2,1,0:T(8,128)(2,1)} %bitcast.78, bf16[1,2048,1024]{2,1,0:T(8,128)(2,1)} %param.23), kind=kOutput, calls=%fused_computation.9 | convolution fusion | flops 2148007936 | bytes 7340032 | tf_op jit(solution)/shard_map/sxcf,xfd->sxcd/dot_general | solution.py:376
  170.8 5.4 %all-to-all-start = ((bf16[8,1,64,1024]{3,2,1,0:T(8,128)(2,1)}), bf16[8,1,64,1024]{3,2,1,0:T(8,128)(2,1)S(1)}, u32[]{:S(2)}, u32[]{:S(2)}) async-start(bf16[8,1,64,1024]{3,2,1,0:T(8,128)(2,1)} %fusion.9), calls=%async_computation | async-start | bytes 2097152 | tf_op jit(solution)/shard_map/all_to_all | solution.py:379
  176.8 12.0 %all-gather.3.cloned.1.call-done = bf16[512,2048]{1,0:T(8,128)(2,1)} async-done(((bf16[512,512]{1,0:T(8,128)(2,1)}), bf16[512,2048]{1,0:T(8,128)(2,1)}) %all-gather.3.cloned.1.call-update) | async-done | bytes 2097168 | tf_op jit(solution)/shard_map/all_gather | solution.py:370
  188.8 6.1 %convolution_convert_fusion = bf16[512,1024]{1,0:T(8,128)(2,1)} fusion(bf16[512,2048]{1,0:T(8,128)(2,1)} %all-gather.3.cloned.1.call-done, bf16[2048,1024]{1,0:T(8,128)(2,1)} %param.16), kind=kOutput, calls=%fused_computation.8 | convolution fusion | flops 2148007936 | bytes 7340032 | tf_op jit(solution)/shard_map/dot_general | solution.py:369
  194.9 5.5 %all-to-all-done = bf16[8,1,64,1024]{3,2,1,0:T(8,128)(2,1)S(1)} async-done(((bf16[8,1,64,1024]{3,2,1,0:T(8,128)(2,1)}), bf16[8,1,64,1024]{3,2,1,0:T(8,128)(2,1)S(1)}, u32[]{:S(2)}, u32[]{:S(2)}) %all-to-all-start) | async-done | bytes 1048608 | tf_op jit(solution)/shard_map/all_to_all | solution.py:379
  200.4 1.2 gather_fusion
  201.8 2.3 %multiply_reduce_fusion = bf16[128,1024]{1,0:T(8,128)(2,1)} fusion(bf16[128,2,1024]{2,1,0:T(2,128)(2,1)S(1)} %gather.7, pred[128,2]{1,0:T(8,128)(4,1)S(1)} %copy.40, f32[128,2]{1,0:T(8,128)S(1)} %copy.43), kind=kLoop, calls=%fused_computation.14 | loop fusion | flops 917504 | bytes 787712 | tf_op jit(solution)/shard_map/reduce_sum | solution.py:383
  (40 shorter events, 1.9 us)
Async XLA Ops:
  7.2 157.5 %all-gather.5.cloned.1.call-start = ((), (), s32[]{:S(2)}) async-start(), calls=%async_computation.2 | async-start | bytes 2621440 | tf_op jit(solution)/shard_map/all_gather | solution.py:374
  16.3 1.0 copy-start
  17.3 1.0 copy-start.1
  18.3 1.0 copy-start.2
  19.4 90.3 %copy-start.5 = (bf16[1,4096,512]{2,1,0:T(8,128)(2,1)S(1)}, bf16[1,4096,512]{2,1,0:T(8,128)(2,1)}, u32[]{:S(2)}) copy-start(bf16[1,4096,512]{2,1,0:T(8,128)(2,1)} %param.21) | copy-start | bytes 12582916
  109.7 2.3 %copy-start.6 = (bf16[1,4096,512]{2,1,0:T(8,128)(2,1)S(1)}, bf16[1,4096,512]{2,1,0:T(8,128)(2,1)}, u32[]{:S(2)}) copy-start(bf16[1,4096,512]{2,1,0:T(8,128)(2,1)} %param.22) | copy-start | bytes 12582916
  115.3 73.5 %all-gather.3.cloned.1.call-start = ((), (), s32[]{:S(2)}) async-start(), calls=%async_computation.1 | async-start | bytes 2621440 | tf_op jit(solution)/shard_map/all_gather | solution.py:370
  164.6 11.8 %copy-start.3 = (s32[128,2]{0,1:T(2,128)S(1)}, s32[128,2]{0,1:T(2,128)}, u32[]{:S(2)}) copy-start(s32[128,2]{0,1:T(2,128)} %param.19) | copy-start | bytes 3076
  164.6 12.0 %copy-start.4 = (f32[128,2]{0,1:T(2,128)S(1)}, f32[128,2]{0,1:T(2,128)}, u32[]{:S(2)}) copy-start(f32[128,2]{0,1:T(2,128)} %param.20) | copy-start | bytes 3076
  170.8 29.6 %all-to-all-start = ((bf16[8,1,64,1024]{3,2,1,0:T(8,128)(2,1)}), bf16[8,1,64,1024]{3,2,1,0:T(8,128)(2,1)S(1)}, u32[]{:S(2)}, u32[]{:S(2)}) async-start(bf16[8,1,64,1024]{3,2,1,0:T(8,128)(2,1)} %fusion.9), calls=%async_computation | async-start | bytes 2097152 | tf_op jit(solution)/shard_map/all_to_all | solution.py:379
Sparse Core Ops, SparseCore 0:
  115.4 49.1 all-gather.4
  166.2 22.5 all-gather.2
where the time goes:
time: 215 us; the launch traced here: 211 us
  Pallas kernels  90.3 us (42%)
  waiting for transfers between devices  66.8 us (31%)
  matrix products  17.8 us (8%)
  between operations  14.3 us (7%)
  other arithmetic  8.92 us (4%)
  local copies, waits for them, and re-layouts  7.37 us (3%)
  starting transfers between devices  5.52 us (3%)
    pallas_call x1, Pallas kernels, attention(): pl.pallas_call(functools.partial(attention_kernel, n, tp, heads), out_sha...  90.3 us
    all_gather x1, waiting for transfers between devices, body(): part_rows = lax.all_gather(flat_hidden, 'tp', axis=1, tiled=True)  48.6 us
    all_gather x1, waiting for transfers between devices, body(): lax.all_gather(attended, 'tp', axis=1, tiled=True)  12 us
    dot_general x1, matrix products, body(): jnp.einsum('sxcf,xfd->sxcd', shaped, down_weight, preferred_element_type=...  6.15 us
    dot_general x1, matrix products, body(): jnp.dot(lax.all_gather(attended, 'tp', axis=1, tiled=True), out_weight, p...  6.12 us
    all_to_all x1, waiting for transfers between devices, body(): lax.all_to_all(leaving, 'ep', split_axis=0, concat_axis=0, tiled=True)  5.46 us
    all_to_all x1, starting transfers between devices, body(): lax.all_to_all(leaving, 'ep', split_axis=0, concat_axis=0, tiled=True)  5.44 us
  transfers between devices with their start and end apart: 3, of which 3 were waited for; matrix products, arithmetic and copies ran while one was open for 6% of the time, Pallas kernels for 0%

commit v1 on v0

--- a/solution.py
+++ b/solution.py
@@ -316,7 +316,7 @@
     return entries * capacity + ranking
 
 
-def body(
+def staged(
     queries,
     key_rows,
     values,
@@ -386,6 +386,632 @@
     return (mixer_sum.astype(jnp.bfloat16), combined.astype(jnp.bfloat16))
 
 
+def fused_kernel(
+    n, tp, heads, cores, q_ref, k_ref, v_ref, gate_ref, x_ref, gain_ref, ids_ref, mix_ref,
+    wg_ref, wu_ref, wd_ref, wo_ref,
+    mixed_ref, expert_ref,
+    wg, wu, wd, wo, x_buf, token_buf, leave_buf, routed, hidden, product, back, comb_hi, comb_lo,
+    k_buf, v_buf, q_buf, o_buf, own_buf, own_lse, part_buf, part_lse, got_buf, got_lse, attended,
+    load, send_k, recv_k, send_v, recv_v, send_q, recv_q, send_o, recv_o,
+    send_p, recv_p, send_l, recv_l, send_t, recv_t, send_a, recv_a, send_f, recv_f,
+    send_h, recv_h, send_r, recv_r, send_m, recv_m,
+):
+    groups = n // heads
+    chips = tp // cores
+    rows = k_ref.shape[0]
+    width = k_ref.shape[1] // heads
+    halves = q_buf.shape[1]
+    chunk = rows // halves
+    tokens, depth = x_ref.shape
+    share = leave_buf.shape[0] // n
+    capacity = share * tp
+    block_rows = token_buf.shape[0]
+    chosen = ids_ref.shape[0]
+    inner = wg.shape[1]
+    out_width = wo.shape[1]
+    factor = LOG2E * width ** (-0.5)
+    me, my_tp = lax.axis_index("ep"), lax.axis_index("tp")
+    my_group, my_head = me // heads, me % heads
+    my_chip, my_core = my_tp // cores, my_tp % cores
+    base = my_group * heads
+
+    siblings = [my_chip * cores + (my_core + s) % cores for s in range(1, cores)]
+    across = [((my_chip + s) % chips) * cores + my_core for s in range(1, chips)]
+    rest = [
+        ((my_chip + s) % chips) * cores + (my_core + r) % cores
+        for s in range(1, chips) for r in range(1, cores)
+    ]
+
+    def span(start, size):
+        return pl.ds(pl.multiple_of(start * size, size), size)
+
+    def arrived(ref, sem):
+        pltpu.make_async_copy(ref, ref, sem).wait()
+
+    def to_ep(src, dst, send, recv, target):
+        return pltpu.make_async_remote_copy(
+            src_ref=src, dst_ref=dst, send_sem=send, recv_sem=recv, device_id={"ep": target}
+        )
+
+    def gather(piece, sends, recvs, first):
+        def copy(owner, target):
+            return pltpu.make_async_remote_copy(
+                src_ref=piece(owner), dst_ref=piece(owner), send_sem=sends.at[first + owner, target],
+                recv_sem=recvs.at[first + owner], device_id={"tp": target},
+            )
+
+        def start():
+            for target in across + siblings:
+                copy(my_tp, target).start()
+
+        def forward():
+            for owner in across:
+                arrived(piece(owner), recvs.at[first + owner])
+                for target in siblings:
+                    copy(owner, target).start()
+
+        def finish():
+            for owner in siblings + rest:
+                arrived(piece(owner), recvs.at[first + owner])
+
+        def drain():
+            for target in across + siblings:
+                copy(my_tp, target).wait_send()
+            for owner in across:
+                for target in siblings:
+                    copy(owner, target).wait_send()
+
+        return start, forward, finish, drain
+
+    def token_piece(owner):
+        return token_buf.at[span(owner, tokens), :]
+
+    def routed_piece(source):
+        return lambda owner: routed.at[span(source * tp + owner, share), :]
+
+    parts = send_h.shape[0] // tp
+    strip = inner // parts
+
+    def hidden_piece(part):
+        return lambda owner: hidden.at[:, span(owner * parts + part, strip)]
+
+    def mixed_piece(head):
+        return lambda owner: attended.at[:, span(owner * heads + head, width)]
+
+    token_gather = gather(token_piece, send_t, recv_t, 0)
+
+    def spread(source):
+        return gather(routed_piece(source), send_f, recv_f, source * tp)
+
+    def hidden_gather(part):
+        return gather(hidden_piece(part), send_h, recv_h, part * tp)
+
+    def mixed_gather(head):
+        return gather(mixed_piece(head), send_m, recv_m, head * tp)
+
+    loads = [
+        pltpu.make_async_copy(src, dst, load.at[i])
+        for i, (src, dst) in enumerate((
+            (x_ref, x_buf), (wg_ref.at[0], wg), (wu_ref.at[0], wu), (wd_ref.at[0], wd), (wo_ref, wo),
+        ))
+    ]
+    loads[0].start()
+
+    barrier = pltpu.get_barrier_semaphore()
+
+    @pl.loop(1, n)
+    def _(step):
+        pl.semaphore_signal(barrier, inc=1, device_id={"ep": (me + step) % n})
+
+    @pl.loop(1, tp)
+    def _(step):
+        pl.semaphore_signal(barrier, inc=1, device_id={"tp": (my_tp + step) % tp})
+
+    loads[0].wait()
+    as_float = x_buf[...].astype(jnp.float32)
+    center = jnp.mean(as_float, axis=1, keepdims=True)
+    shifted = as_float - center
+    variance = jnp.mean(jnp.square(shifted), axis=1, keepdims=True)
+    token_buf[span(my_tp, tokens), :] = (
+        shifted * lax.rsqrt(variance + EPSILON) * gain_ref[...]
+    ).astype(token_buf.dtype)
+
+    pl.semaphore_wait(barrier, n + tp - 2)
+    token_gather[0]()
+
+    def kv_copies(head):
+        cols = span(head, width)
+        target = base + head
+        return (
+            to_ep(k_ref.at[:, cols], k_buf.at[my_head], send_k.at[head], recv_k.at[my_head], target),
+            to_ep(v_ref.at[:, cols], v_buf.at[my_head], send_v.at[head], recv_v.at[my_head], target),
+        )
+
+    def q_copy(group, head, half):
+        target = group * heads + head
+        return to_ep(
+            q_ref.at[span(half, chunk), span(head, width)], q_buf.at[me, half],
+            send_q.at[target, half], recv_q.at[me, half], target,
+        )
+
+    own_cols = span(my_head, width)
+    keep_k = pltpu.make_async_copy(k_ref.at[:, own_cols], k_buf.at[my_head], recv_k.at[my_head])
+    keep_v = pltpu.make_async_copy(v_ref.at[:, own_cols], v_buf.at[my_head], recv_v.at[my_head])
+    keep_k.start()
+    keep_v.start()
+    for half in range(halves):
+        pltpu.make_async_copy(
+            q_ref.at[span(half, chunk), own_cols], q_buf.at[me, half], recv_q.at[me, half]
+        ).start()
+
+    def lower_queries(half):
+        @pl.loop(0, my_group)
+        def _(group):
+            @pl.loop(0, heads)
+            def _(step):
+                q_copy(group, (my_head + step) % heads, half).start()
+
+    @pl.loop(1, heads)
+    def _(step):
+        for copy in kv_copies((my_head + step) % heads):
+            copy.start()
+
+    lower_queries(0)
+
+    @pl.loop(1, heads)
+    def _(step):
+        for half in range(halves):
+            q_copy(my_group, (my_head + step) % heads, half).start()
+
+    for copy in loads[1:]:
+        copy.start()
+
+    expert = lax.broadcasted_iota(jnp.int32, (n, block_rows), 0)
+    named = jnp.zeros((n, block_rows), jnp.float32)
+    scale = jnp.zeros((n, block_rows), jnp.float32)
+    for k in range(chosen):
+        match = expert == ids_ref[k : k + 1, :]
+        named = jnp.where(match, 1.0, named)
+        scale = jnp.where(match, mix_ref[k : k + 1, :], scale)
+    before = lax.broadcasted_iota(jnp.int32, (block_rows, block_rows), 0)
+    after = lax.broadcasted_iota(jnp.int32, (block_rows, block_rows), 1)
+    ranks = jnp.dot(
+        named.astype(jnp.bfloat16), jnp.where(before < after, 1.0, 0.0).astype(jnp.bfloat16),
+        preferred_element_type=jnp.float32,
+    )
+
+    def per_slot(table, count):
+        return jnp.broadcast_to(table[:, None, :], (n, count, block_rows))
+
+    slots = lax.broadcasted_iota(jnp.int32, (n, share, block_rows), 1) + my_tp * share
+    picks = jnp.where(
+        per_slot(ranks, share) == slots.astype(jnp.float32), per_slot(named, share), 0.0
+    ).reshape(n * share, block_rows).astype(jnp.bfloat16)
+
+    token_gather[1]()
+    token_gather[2]()
+
+    piece = depth // 8
+
+    @pl.loop(0, depth // piece)
+    def _(i):
+        cols = span(i, piece)
+        leave_buf[:, cols] = jnp.dot(
+            picks, token_buf[:, cols], preferred_element_type=jnp.float32
+        ).astype(leave_buf.dtype)
+
+    def leave_copy(target):
+        return to_ep(
+            leave_buf.at[span(target, share), :], routed_piece(me)(my_tp),
+            send_a.at[target], recv_a.at[me], target,
+        )
+
+    pltpu.make_async_copy(
+        leave_buf.at[span(me, share), :], routed_piece(me)(my_tp), recv_a.at[me]
+    ).start()
+
+    @pl.loop(1, n)
+    def _(step):
+        leave_copy((me + step) % n).start()
+
+    lower_queries(1)
+
+    all_slots = lax.broadcasted_iota(jnp.int32, (n, capacity, block_rows), 1)
+    comb = jnp.where(
+        per_slot(ranks, capacity) == all_slots.astype(jnp.float32), per_slot(scale, capacity), 0.0
+    ).reshape(n * capacity, block_rows)
+    comb = jnp.where(
+        jnp.broadcast_to(named[:, None, :], (n, capacity, block_rows)).reshape(
+            n * capacity, block_rows) > 0.0, comb, 0.0
+    ).T
+    high = comb.astype(jnp.bfloat16)
+    comb_hi[...] = high
+    comb_lo[...] = (comb - high.astype(jnp.float32)).astype(jnp.bfloat16)
+
+    @pl.loop(0, heads)
+    def _(step):
+        source = (my_head + step) % heads
+        arrived(k_buf.at[source], recv_k.at[source])
+        arrived(v_buf.at[source], recv_v.at[source])
+
+    def key_gate(source):
+        return gate_ref[pl.ds(my_head, 1), span(base + source, rows)] * LOG2E
+
+    def line_gate(i, half):
+        line = gate_ref[pl.ds(my_head, 1), span(i * halves + half, chunk)] * LOG2E
+        return jnp.broadcast_to(line, (width, chunk)).T[:, :1]
+
+    def attend(i, half, first, count, causal):
+        query = q_buf[i, half]
+        gate = line_gate(i, half)
+
+        def scores_of(source):
+            raw = lax.dot_general(
+                query, k_buf[source], (((1,), (1,)), ((), ())), preferred_element_type=jnp.float32
+            )
+            return raw * factor - key_gate(source)
+
+        def weigh(weights, source):
+            return jnp.dot(
+                weights.astype(jnp.bfloat16), v_buf[source], preferred_element_type=jnp.float32
+            )
+
+        scores = scores_of(first)
+        if causal:
+            column = lax.broadcasted_iota(jnp.int32, (chunk, rows), 1)
+            line = lax.broadcasted_iota(jnp.int32, (chunk, rows), 0) + half * chunk
+            scores = jnp.where(column <= line, scores, -jnp.inf)
+        top = jnp.max(scores, axis=1, keepdims=True) + gate
+        weights = jnp.exp2(scores - (top - gate))
+        total = jnp.sum(weights, axis=1, keepdims=True)
+        held = weigh(weights, first)
+
+        def fold(source, state):
+            top, total, held = state
+            scores = scores_of(source)
+            newest = jnp.maximum(top, jnp.max(scores, axis=1, keepdims=True) + gate)
+            shrink = jnp.exp2(top - newest)
+            weights = jnp.exp2(scores - (newest - gate))
+            total = total * shrink + jnp.sum(weights, axis=1, keepdims=True)
+            held = held * shrink + weigh(weights, source)
+            return newest, total, held
+
+        top, total, held = lax.fori_loop(0, count, fold, (top, total, held))
+        return held / total, top + jnp.log(total) * LOG2E
+
+    def back_copy(source, half):
+        return to_ep(
+            o_buf.at[source, half], attended.at[span(half, chunk), span(my_tp * heads + my_head, width)],
+            send_o.at[source, half], recv_o.at[my_head, half], base + source,
+        )
+
+    def give(source, half):
+        @pl.when(source != my_head)
+        def _():
+            back_copy(source, half).start()
+
+        @pl.when(source == my_head)
+        def _():
+            pltpu.make_async_copy(
+                o_buf.at[source, half],
+                attended.at[span(half, chunk), span(my_tp * heads + my_head, width)],
+                recv_o.at[my_head, half],
+            ).start()
+
+    def spread_step(step):
+        source = (me + n - step) % n
+        arrived(routed_piece(source)(my_tp), recv_a.at[source])
+        spread(source)[0]()
+
+    per_head = n // heads
+
+    @pl.loop(0, heads)
+    def _(source):
+        for half in range(halves):
+            i = base + source
+            arrived(q_buf.at[i, half], recv_q.at[i, half])
+            out, lse = attend(i, half, source, source, True)
+
+            @pl.when(my_group == 0)
+            def _():
+                o_buf[source, half] = out.astype(o_buf.dtype)
+                give(source, half)
+
+            @pl.when(my_group > 0)
+            def _():
+                own_buf[source, half] = out
+                own_lse[source, half] = jnp.broadcast_to(lse, (chunk, width))
+
+        for s in range(per_head):
+            spread_step(source * per_head + s)
+
+    def part_copies(i, half):
+        slot = i % heads
+        return (
+            to_ep(part_buf.at[i, half], got_buf.at[my_group, slot, half],
+                  send_p.at[i, half], recv_p.at[my_group, slot * halves + half],
+                  (i // heads) * heads + my_head),
+            to_ep(part_lse.at[i, half], got_lse.at[my_group, slot, half],
+                  send_l.at[i, half], recv_l.at[my_group, slot * halves + half],
+                  (i // heads) * heads + my_head),
+        )
+
+    def later_queries(half):
+        @pl.loop(base + heads, n)
+        def _(i):
+            arrived(q_buf.at[i, half], recv_q.at[i, half])
+            out, lse = attend(i, half, heads - 1, heads - 1, False)
+            part_buf[i, half] = out.astype(part_buf.dtype)
+            part_lse[i, half] = jnp.broadcast_to(lse, (chunk, width)).T[: part_lse.shape[2], :]
+            for copy in part_copies(i, half):
+                copy.start()
+
+    later_queries(0)
+
+    @pl.loop(0, n)
+    def _(step):
+        spread((me + n - step) % n)[1]()
+
+    @pl.loop(0, n)
+    def _(step):
+        spread((me + n - step) % n)[2]()
+
+    loads[1].wait()
+    loads[2].wait()
+    for part in range(parts):
+        cols = slice(part * strip, (part + 1) * strip)
+        gate_part = jnp.dot(routed[...], wg[:, cols], preferred_element_type=jnp.float32)
+        up_part = jnp.dot(routed[...], wu[:, cols], preferred_element_type=jnp.float32)
+        hidden[:, span(my_tp * parts + part, strip)] = (
+            gate_part / (1.0 + jnp.exp(-gate_part)) * up_part
+        ).astype(hidden.dtype)
+        hidden_gather(part)[0]()
+
+    later_queries(1)
+
+    for part in range(parts):
+        hidden_gather(part)[1]()
+
+    def merge(half):
+        @pl.when(my_group > 0)
+        def _():
+            @pl.loop(0, heads)
+            def _(source):
+                @pl.loop(0, my_group)
+                def _(group):
+                    place = source * halves + half
+                    arrived(got_buf.at[group, source, half], recv_p.at[group, place])
+                    arrived(got_lse.at[group, source, half], recv_l.at[group, place])
+                    line = got_lse[group, source, half][:1, :]
+                    theirs = jnp.broadcast_to(line, (width, chunk)).T
+                    mine = own_lse[source, half]
+                    top = jnp.maximum(mine, theirs)
+                    a, b = jnp.exp2(mine - top), jnp.exp2(theirs - top)
+                    total = a + b
+                    own_buf[source, half] = (
+                        own_buf[source, half] * a
+                        + got_buf[group, source, half].astype(jnp.float32) * b
+                    ) / total
+                    own_lse[source, half] = top + jnp.log(total) * LOG2E
+
+                o_buf[source, half] = own_buf[source, half].astype(o_buf.dtype)
+                give(source, half)
+
+    merge(0)
+
+    for part in range(parts):
+        hidden_gather(part)[2]()
+    loads[3].wait()
+    tiles = 2
+    tall = n * capacity // tiles
+    each = n // tiles
+
+    def return_copy(target):
+        return to_ep(
+            product.at[span(target, capacity), :], back.at[span(me, capacity), :],
+            send_r.at[target], recv_r.at[me], target,
+        )
+
+    @pl.loop(0, tiles)
+    def _(step):
+        tile = (step + 1 + me // each) % tiles
+        lines = span(tile, tall)
+        product[lines, :] = jnp.dot(
+            hidden[lines, :], wd[...], preferred_element_type=jnp.float32
+        ).astype(product.dtype)
+
+        @pl.loop(0, each)
+        def _(place):
+            target = tile * each + (place + me) % each
+
+            @pl.when(target != me)
+            def _():
+                return_copy(target).start()
+
+            @pl.when(target == me)
+            def _():
+                pltpu.make_async_copy(
+                    product.at[span(me, capacity), :], back.at[span(me, capacity), :], recv_r.at[me]
+                ).start()
+
+    for half in range(1, halves):
+        merge(half)
+
+    @pl.loop(0, heads)
+    def _(step):
+        head = (my_head + step) % heads
+        for half in range(halves):
+            arrived(
+                attended.at[span(half, chunk), span(my_tp * heads + head, width)],
+                recv_o.at[head, half],
+            )
+        mixed_gather(head)[0]()
+
+    @pl.loop(0, heads)
+    def _(step):
+        mixed_gather((my_head + step) % heads)[1]()
+
+    @pl.loop(0, heads)
+    def _(head):
+        mixed_gather(head)[2]()
+
+    loads[4].wait()
+
+    @pl.loop(0, 2)
+    def _(step):
+        lines = span(step, rows // 2)
+        mixed_ref[lines, :] = jnp.dot(
+            attended[lines, :], wo[...], preferred_element_type=jnp.float32
+        ).astype(mixed_ref.dtype)
+
+    @pl.loop(0, n)
+    def _(source):
+        arrived(back.at[span(source, capacity), :], recv_r.at[source])
+
+    expert_ref[...] = (
+        jnp.dot(comb_hi[...], back[...], preferred_element_type=jnp.float32)
+        + jnp.dot(comb_lo[...], back[...], preferred_element_type=jnp.float32)
+    ).astype(expert_ref.dtype)
+
+    token_gather[3]()
+
+    @pl.loop(1, heads)
+    def _(step):
+        head = (my_head + step) % heads
+        for copy in kv_copies(head):
+            copy.wait_send()
+        for half in range(halves):
+            q_copy(my_group, head, half).wait_send()
+            back_copy(head, half).wait_send()
+
+    @pl.loop(0, my_group)
+    def _(group):
+        @pl.loop(0, heads)
+        def _(head):
+            for half in range(halves):
+                q_copy(group, head, half).wait_send()
+
+    @pl.loop(base + heads, n)
+    def _(i):
+        for half in range(halves):
+            for copy in part_copies(i, half):
+                copy.wait_send()
+
+    @pl.loop(1, n)
+    def _(step):
+        leave_copy((me + step) % n).wait_send()
+        return_copy((me + step) % n).wait_send()
+
+    @pl.loop(0, n)
+    def _(source):
+        spread(source)[3]()
+
+    for part in range(parts):
+        hidden_gather(part)[3]()
+
+    @pl.loop(0, heads)
+    def _(head):
+        mixed_gather(head)[3]()
+
+
+def fused(
+    cores, queries, key_rows, values, forget_log, out_weight, expert_input, norm_gain, route_ids,
+    route_weights, gate_weight, up_weight, down_weight,
+):
+    n, tp = lax.axis_size("ep"), lax.axis_size("tp")
+    rows, heads = queries.shape[0], forget_log.shape[1]
+    width = queries.shape[1] // heads
+    groups, halves, parts = n // heads, 2, 2
+    chunk = rows // halves
+    tokens, depth = expert_input.shape
+    block_rows, chosen = route_ids.shape
+    capacity = block_rows * chosen * 2 // n
+    share = capacity // tp
+    slots = n * capacity
+    inner, out_width = gate_weight.shape[2], out_weight.shape[1]
+    half_type, wide = jnp.bfloat16, jnp.float32
+    vmem, hbm = pl.BlockSpec(memory_space=pltpu.VMEM), pl.BlockSpec(memory_space=pl.ANY)
+    dma = pltpu.SemaphoreType.DMA
+    blocks = n * n // 2
+    return pl.pallas_call(
+        functools.partial(fused_kernel, n, tp, heads, cores),
+        out_shape=(
+            jax.ShapeDtypeStruct((rows, out_width), half_type),
+            jax.ShapeDtypeStruct((block_rows, out_width), half_type),
+        ),
+        in_specs=[hbm, hbm, hbm, vmem, hbm, vmem, vmem, vmem, hbm, hbm, hbm, hbm],
+        out_specs=(vmem, vmem),
+        scratch_shapes=[
+            pltpu.VMEM((depth, inner), half_type), pltpu.VMEM((depth, inner), half_type),
+            pltpu.VMEM((inner * tp, out_width), half_type),
+            pltpu.VMEM((width * heads * tp, out_width), half_type),
+            pltpu.VMEM((tokens, depth), half_type), pltpu.VMEM((block_rows, depth), half_type),
+            pltpu.VMEM((n * share, depth), half_type), pltpu.VMEM((slots, depth), half_type),
+            pltpu.VMEM((slots, inner * tp), half_type), pltpu.VMEM((slots, out_width), half_type),
+            pltpu.VMEM((slots, out_width), half_type),
+            pltpu.VMEM((block_rows, slots), half_type), pltpu.VMEM((block_rows, slots), half_type),
+            pltpu.VMEM((heads, rows, width), half_type), pltpu.VMEM((heads, rows, width), half_type),
+            pltpu.VMEM((n, halves, chunk, width), half_type),
+            pltpu.VMEM((heads, halves, chunk, width), half_type),
+            pltpu.VMEM((heads, halves, chunk, width), wide),
+            pltpu.VMEM((heads, halves, chunk, width), wide),
+            pltpu.VMEM((n, halves, chunk, width), half_type),
+            pltpu.VMEM((n, halves, 8, chunk), wide),
+            pltpu.VMEM((groups, heads, halves, chunk, width), half_type),
+            pltpu.VMEM((groups, heads, halves, 8, chunk), wide),
+            pltpu.VMEM((rows, width * heads * tp), half_type),
+            dma((5,)), dma((heads,)), dma((heads,)), dma((heads,)), dma((heads,)),
+            dma((n, halves)), dma((n, halves)), dma((heads, halves)), dma((heads, halves)),
+            dma((n, halves)), dma((groups, heads * halves)),
+            dma((n, halves)), dma((groups, heads * halves)),
+            dma((tp, tp)), dma((tp,)), dma((n,)), dma((n,)), dma((n * tp, tp)), dma((n * tp,)),
+            dma((parts * tp, tp)), dma((parts * tp,)), dma((n,)), dma((n,)),
+            dma((heads * tp, tp)), dma((heads * tp,)),
+        ],
+        compiler_params=pltpu.CompilerParams(
+            collective_id=0, has_side_effects=True, vmem_limit_bytes=58 * 1024 * 1024
+        ),
+        cost_estimate=pl.CostEstimate(
+            flops=6 * slots * depth * inner + 2 * rows * rows * width * blocks,
+            bytes_accessed=8 * depth * inner, transcendentals=blocks * rows * rows,
+        ),
+    )(
+        queries, key_rows, values, forget_log.T, expert_input, norm_gain.reshape(1, depth),
+        route_ids.T, route_weights.T, gate_weight, up_weight, down_weight, out_weight,
+    )
+
+
+def chip_cores(mesh):
+    names = list(mesh.axis_names)
+    line = mesh.devices.transpose(names.index("ep"), names.index("tp"))[0]
+    spots = [getattr(device, "coords", i) for i, device in enumerate(line)]
+    spots = [tuple(spot) if hasattr(spot, "__len__") else spot for spot in spots]
+    cores = sum(spot == spots[0] for spot in spots)
+    even = len(spots) % cores == 0 and all(
+        spots[i] == spots[i - i % cores] for i in range(len(spots))
+    )
+    return cores if even else 1
+
+
+def fits(n, tp, heads, block_rows, chosen, local_experts, inner):
+    capacity = block_rows * chosen * 2 // (n * local_experts)
+    return (
+        local_experts == 1 and n % heads == 0 and heads > 1 and capacity % (16 * tp) == 0
+        and n % 2 == 0 and inner % 256 == 0
+    )
+
+
+def choose(cores, *args):
+    n, tp = lax.axis_size("ep"), lax.axis_size("tp")
+    ids, gate_weight = args[7], args[9]
+    if fits(
+        n, tp, args[3].shape[1], ids.shape[0], ids.shape[1], gate_weight.shape[0],
+        gate_weight.shape[2],
+    ):
+        return fused(cores, *args)
+    return staged(*args)
+
+
 def solution(mesh):
     placed = (
         P("ep", "tp"),
@@ -402,5 +1028,5 @@
         P("ep", None, "tp"),
     )
     return jax.shard_map(
-        body, mesh=mesh, in_specs=placed, out_specs=(P("ep", "tp"), P("ep", "tp")), check_vma=False
-    )
+        functools.partial(choose, chip_cores(mesh)), mesh=mesh, in_specs=placed, out_specs=(P("ep", "tp"), P("ep", "tp")), check_vma=False
+    )

time: 215 us -> 126 us (0.59); the launches traced: 211 us -> 126 us
  waiting for transfers between devices: 66.8 us -> 0 us
  Pallas kernels: 90.3 us -> 121 us
  matrix products: 17.8 us -> 0 us
  between operations: 14.3 us -> 0.64 us
  other arithmetic: 8.92 us -> 0 us
  starting transfers between devices: 5.52 us -> 0 us
  local copies, waits for them, and re-layouts: 7.37 us -> 3.93 us
    all_gather x2 -> x0, waiting for transfers between devices: 60.6 us -> none  [the longest x1 48.6 us: body(): part_rows = lax.all_gather(flat_hidden, 'tp', axis=1, tiled=True)]
    pallas_call x1, Pallas kernels: 90.3 us -> 121 us  [fused(): pl.pallas_call(functools.partial(fused_kernel, n, tp, heads, cores), out_...]
    dot_general x4 -> x0, matrix products: 17.8 us -> none  [the longest x1 6.15 us: body(): jnp.einsum('sxcf,xfd->sxcd', shaped, down_weight, preferred_element_type=...]
    all_to_all x1 -> x0, waiting for transfers between devices: 5.46 us -> none  [body(): lax.all_to_all(leaving, 'ep', split_axis=0, concat_axis=0, tiled=True)]
    all_to_all x1 -> x0, starting transfers between devices: 5.44 us -> none  [body(): lax.all_to_all(leaving, 'ep', split_axis=0, concat_axis=0, tiled=True)]
    reduce_sum x4 -> x0, other arithmetic: 4.72 us -> none  [the longest x1 2.34 us: body(): jnp.sum((picked * route_weights.reshape(-1)[:, None]).reshape(block_rows,...]
    mul x3 -> x0, other arithmetic: 2.25 us -> none  [the longest x1 1.54 us: attention(): gates = lax.dynamic_slice_in_dim(forget_log.T * LOG2E, me // members, 1, 0)]
  transfers between devices with their start and end apart: 3 -> 0, of which waited for: 3 -> 0; matrix products, arithmetic and copies ran while one was open for 6% -> 0% of each run, Pallas kernels for 0% -> 0%
where the time goes in v1:
time: 126 us
  Pallas kernels  121 us (96%)
  local copies, waits for them, and re-layouts  3.93 us (3%)
    pallas_call x1, Pallas kernels, fused(): pl.pallas_call(functools.partial(fused_kernel, n, tp, heads, cores), out_...  121 us
    unnamed x2, local copies, waits for them, and re-layouts  3.93 us

profile of v1, /device:TPU:27, one launch (start us, length us, event | category | flops | bytes accessed | tf_op | source)
XLA Modules:
  0.0 125.8 jit_solution(15465820486004695064)
XLA Ops:
  0.6 121.2 %shard_map.131 = (bf16[512,1024]{1,0:T(8,128)(2,1)}, bf16[128,1024]{1,0:T(8,128)(2,1)}) custom-call(bf16[512,512]{1,0:T(8,128)(2,1)} %q_ref.1, bf16[512,512]{1,0:T(8,128)(2,1)} %k_ref.1, bf16[512,512]{1,0:T(8,128)(2,1)} %v_ref.1, f32[4,4096]{1,0:T(4,128)} %bitcast.4, bf16[32,4096]{1,0:T(8,128)(2,1)} %x_ref.1, f32[1,4096]{1,0:T(1,128)} %bitcast.5, ...), custom_call_target="tpu_custom_call" | custom-call | flops 8589934592 | bytes 16777216 | tf_op jit(solution)/shard_map/pallas_call | solution.py:936
  121.9 2.3 %copy.16 = bf16[512,1024]{1,0:T(8,128)(2,1)} copy(bf16[512,1024]{1,0:T(8,128)(2,1)} %get-tuple-element.4) | data formatting | bytes 2097152
  124.1 1.7 %copy.17 = bf16[128,1024]{1,0:T(8,128)(2,1)} copy(bf16[128,1024]{1,0:T(8,128)(2,1)} %get-tuple-element.5) | data formatting | bytes 524288

commit v2 on v1

--- a/solution.py
+++ b/solution.py
@@ -391,10 +391,12 @@
     wg_ref, wu_ref, wd_ref, wo_ref,
     mixed_ref, expert_ref,
     wg, wu, wd, wo, x_buf, token_buf, leave_buf, routed, hidden, product, back, comb_hi, comb_lo,
+    ids_buf, mix_buf, sums_out, sums_in,
     k_buf, v_buf, q_buf, o_buf, own_buf, own_lse, part_buf, part_lse, got_buf, got_lse, attended,
     load, send_k, recv_k, send_v, recv_v, send_q, recv_q, send_o, recv_o,
     send_p, recv_p, send_l, recv_l, send_t, recv_t, send_a, recv_a, send_f, recv_f,
     send_h, recv_h, send_r, recv_r, send_m, recv_m,
+    send_i, recv_i, send_w, recv_w, send_c, recv_c,
 ):
     groups = n // heads
     chips = tp // cores
@@ -475,8 +477,8 @@
     def hidden_piece(part):
         return lambda owner: hidden.at[:, span(owner * parts + part, strip)]
 
-    def mixed_piece(head):
-        return lambda owner: attended.at[:, span(owner * heads + head, width)]
+    def mixed_piece(half):
+        return lambda owner: attended.at[span(half, chunk), span(owner, heads * width)]
 
     token_gather = gather(token_piece, send_t, recv_t, 0)
 
@@ -486,8 +488,20 @@
     def hidden_gather(part):
         return gather(hidden_piece(part), send_h, recv_h, part * tp)
 
-    def mixed_gather(head):
-        return gather(mixed_piece(head), send_m, recv_m, head * tp)
+    def mixed_gather(half):
+        return gather(mixed_piece(half), send_m, recv_m, half * tp)
+
+    across_groups = [(g, (heads // 2 + s) % heads) for g in range(1, groups) for s in range(heads)]
+    in_group = [(0, s) for s in range(1, heads)]
+    order = [(0, 0)]
+    for place in range(max(len(across_groups), len(in_group))):
+        order += across_groups[place : place + 1] + in_group[place : place + 1]
+
+    def peer(step, sign):
+        group, head = order[step]
+        return ((my_group + groups + sign * group) % groups) * heads + (
+            my_head + heads + sign * head
+        ) % heads
 
     loads = [
         pltpu.make_async_copy(src, dst, load.at[i])
@@ -516,32 +530,55 @@
         shifted * lax.rsqrt(variance + EPSILON) * gain_ref[...]
     ).astype(token_buf.dtype)
 
+    ids_buf[my_group] = ids_ref[...]
+    mix_buf[my_group] = mix_ref[...]
     pl.semaphore_wait(barrier, n + tp - 2)
     token_gather[0]()
+    others = [(my_group + step) % groups for step in range(1, groups)]
+
+    def route_copies(group):
+        target = group * heads + my_head
+        return (
+            to_ep(ids_ref, ids_buf.at[my_group], send_i.at[group], recv_i.at[my_group], target),
+            to_ep(mix_ref, mix_buf.at[my_group], send_w.at[group], recv_w.at[my_group], target),
+        )
+
+    for group in others:
+        for copy in route_copies(group):
+            copy.start()
+
+    def k_spot(source):
+        return k_buf.at[span(source, rows), :width]
+
+    def v_spot(source):
+        return v_buf.at[span(source, rows), :width]
+
+    def q_spot(source, half):
+        return q_buf.at[source, half, :, :width]
 
     def kv_copies(head):
         cols = span(head, width)
         target = base + head
         return (
-            to_ep(k_ref.at[:, cols], k_buf.at[my_head], send_k.at[head], recv_k.at[my_head], target),
-            to_ep(v_ref.at[:, cols], v_buf.at[my_head], send_v.at[head], recv_v.at[my_head], target),
+            to_ep(k_ref.at[:, cols], k_spot(my_head), send_k.at[head], recv_k.at[my_head], target),
+            to_ep(v_ref.at[:, cols], v_spot(my_head), send_v.at[head], recv_v.at[my_head], target),
         )
 
     def q_copy(group, head, half):
         target = group * heads + head
         return to_ep(
-            q_ref.at[span(half, chunk), span(head, width)], q_buf.at[me, half],
+            q_ref.at[span(half, chunk), span(head, width)], q_spot(me, half),
             send_q.at[target, half], recv_q.at[me, half], target,
         )
 
     own_cols = span(my_head, width)
-    keep_k = pltpu.make_async_copy(k_ref.at[:, own_cols], k_buf.at[my_head], recv_k.at[my_head])
-    keep_v = pltpu.make_async_copy(v_ref.at[:, own_cols], v_buf.at[my_head], recv_v.at[my_head])
+    keep_k = pltpu.make_async_copy(k_ref.at[:, own_cols], k_spot(my_head), recv_k.at[my_head])
+    keep_v = pltpu.make_async_copy(v_ref.at[:, own_cols], v_spot(my_head), recv_v.at[my_head])
     keep_k.start()
     keep_v.start()
     for half in range(halves):
         pltpu.make_async_copy(
-            q_ref.at[span(half, chunk), own_cols], q_buf.at[me, half], recv_q.at[me, half]
+            q_ref.at[span(half, chunk), own_cols], q_spot(me, half), recv_q.at[me, half]
         ).start()
 
     def lower_queries(half):
@@ -558,34 +595,58 @@
 
     lower_queries(0)
 
-    @pl.loop(1, heads)
-    def _(step):
+    terms = lax.broadcasted_iota(jnp.int32, (width, chunk), 0)
+
+    def gate_columns(block, sign, offset):
+        gate = gate_ref[pl.ds(my_head, 1), span(block, chunk)] * (sign * width**0.5)
+        table = jnp.where((terms >= 3 - offset) & (terms < 6 - offset), 1.0, 0.0)
+        for place in range(offset, offset + 3):
+            piece = gate.astype(jnp.bfloat16).astype(jnp.float32)
+            gate = gate - piece
+            table = jnp.where(terms == place, piece, table)
+        return table.T.astype(jnp.bfloat16)
+
+    v_buf[:, width:] = jnp.ones((heads * rows, width), v_buf.dtype)
+
+    @pl.loop(0, heads * halves)
+    def _(place):
+        k_buf[span(place, chunk), width:] = gate_columns(base * halves + place, -1.0, 3)
+
+    @pl.loop(base, n)
+    def _(i):
         for half in range(halves):
+            q_buf[i, half, :, width:] = gate_columns(i * halves + half, 1.0, 0)
+
+    def group_queries(half):
+        @pl.loop(1, heads)
+        def _(step):
             q_copy(my_group, (my_head + step) % heads, half).start()
+
+    group_queries(0)
 
     for copy in loads[1:]:
         copy.start()
 
-    expert = lax.broadcasted_iota(jnp.int32, (n, block_rows), 0)
-    named = jnp.zeros((n, block_rows), jnp.float32)
-    scale = jnp.zeros((n, block_rows), jnp.float32)
-    for k in range(chosen):
-        match = expert == ids_ref[k : k + 1, :]
-        named = jnp.where(match, 1.0, named)
-        scale = jnp.where(match, mix_ref[k : k + 1, :], scale)
     before = lax.broadcasted_iota(jnp.int32, (block_rows, block_rows), 0)
     after = lax.broadcasted_iota(jnp.int32, (block_rows, block_rows), 1)
-    ranks = jnp.dot(
-        named.astype(jnp.bfloat16), jnp.where(before < after, 1.0, 0.0).astype(jnp.bfloat16),
-        preferred_element_type=jnp.float32,
-    )
+    earlier = jnp.where(before < after, 1.0, 0.0).astype(jnp.bfloat16)
+
+    def places(ids, first, count):
+        expert = lax.broadcasted_iota(jnp.int32, (count, block_rows), 0) + first
+        matches = [expert == ids[k : k + 1, :] for k in range(chosen)]
+        named = functools.reduce(jnp.logical_or, matches)
+        ranks = jnp.dot(
+            jnp.where(named, 1.0, 0.0).astype(jnp.bfloat16), earlier,
+            preferred_element_type=jnp.float32,
+        )
+        return matches, jnp.where(named, ranks, -1.0)
 
     def per_slot(table, count):
-        return jnp.broadcast_to(table[:, None, :], (n, count, block_rows))
+        return jnp.broadcast_to(table[:, None, :], (table.shape[0], count, block_rows))
 
     slots = lax.broadcasted_iota(jnp.int32, (n, share, block_rows), 1) + my_tp * share
     picks = jnp.where(
-        per_slot(ranks, share) == slots.astype(jnp.float32), per_slot(named, share), 0.0
+        per_slot(places(ids_ref[...], 0, n)[1], share) == slots.astype(jnp.float32), 1.0, 0.0
     ).reshape(n * share, block_rows).astype(jnp.bfloat16)
 
     token_gather[1]()
@@ -610,80 +671,85 @@
         leave_buf.at[span(me, share), :], routed_piece(me)(my_tp), recv_a.at[me]
     ).start()
 
-    @pl.loop(1, n)
-    def _(step):
-        leave_copy((me + step) % n).start()
-
-    lower_queries(1)
-
-    all_slots = lax.broadcasted_iota(jnp.int32, (n, capacity, block_rows), 1)
-    comb = jnp.where(
-        per_slot(ranks, capacity) == all_slots.astype(jnp.float32), per_slot(scale, capacity), 0.0
-    ).reshape(n * capacity, block_rows)
-    comb = jnp.where(
-        jnp.broadcast_to(named[:, None, :], (n, capacity, block_rows)).reshape(
-            n * capacity, block_rows) > 0.0, comb, 0.0
-    ).T
-    high = comb.astype(jnp.bfloat16)
-    comb_hi[...] = high
-    comb_lo[...] = (comb - high.astype(jnp.float32)).astype(jnp.bfloat16)
+    for step in range(1, n):
+        leave_copy(peer(step, 1)).start()
+
+    for half in range(1, halves):
+        group_queries(half)
+        lower_queries(half)
+
+    def combining(group):
+        matches, ranks = places(ids_buf[group], base, heads)
+        scale = functools.reduce(
+            jnp.add,
+            [
+                jnp.where(match, mix_buf[group, k : k + 1, :], 0.0)
+                for k, match in enumerate(matches)
+            ],
+        )
+        all_slots = lax.broadcasted_iota(jnp.int32, (heads, capacity, block_rows), 1)
+        comb = jnp.where(
+            per_slot(ranks, capacity) == all_slots.astype(jnp.float32),
+            per_slot(scale, capacity), 0.0,
+        ).reshape(heads * capacity, block_rows).T
+        high = comb.astype(jnp.bfloat16)
+        comb_hi[group] = high
+        comb_lo[group] = (comb - high.astype(jnp.float32)).astype(jnp.bfloat16)
+
+    combining(my_group)
+    for group in others:
+        arrived(ids_buf.at[group], recv_i.at[group])
+        arrived(mix_buf.at[group], recv_w.at[group])
+        combining(group)
 
     @pl.loop(0, heads)
     def _(step):
         source = (my_head + step) % heads
-        arrived(k_buf.at[source], recv_k.at[source])
-        arrived(v_buf.at[source], recv_v.at[source])
-
-    def key_gate(source):
-        return gate_ref[pl.ds(my_head, 1), span(base + source, rows)] * LOG2E
-
-    def line_gate(i, half):
-        line = gate_ref[pl.ds(my_head, 1), span(i * halves + half, chunk)] * LOG2E
-        return jnp.broadcast_to(line, (width, chunk)).T[:, :1]
-
-    def attend(i, half, first, count, causal):
+        arrived(k_spot(source), recv_k.at[source])
+        arrived(v_spot(source), recv_v.at[source])
+
+    stretch = 2 * chunk
+
+    def attend(i, half, keys, causal):
         query = q_buf[i, half]
-        gate = line_gate(i, half)
-
-        def scores_of(source):
-            raw = lax.dot_general(
-                query, k_buf[source], (((1,), (1,)), ((), ())), preferred_element_type=jnp.float32
+
+        def scores_of(lines):
+            return lax.dot_general(
+                query, k_buf[lines, :], (((1,), (1,)), ((), ())), preferred_element_type=jnp.float32
             )
-            return raw * factor - key_gate(source)
-
-        def weigh(weights, source):
-            return jnp.dot(
-                weights.astype(jnp.bfloat16), v_buf[source], preferred_element_type=jnp.float32
-            )
-
-        scores = scores_of(first)
+
+        open_keys = keys - chunk if causal else keys
+        cuts = [
+            slice(cut, min(cut + stretch, open_keys)) for cut in range(0, open_keys, stretch)
+        ]
         if causal:
-            column = lax.broadcasted_iota(jnp.int32, (chunk, rows), 1)
-            line = lax.broadcasted_iota(jnp.int32, (chunk, rows), 0) + half * chunk
+            cuts = [slice(open_keys, keys), *cuts]
+        scores = scores_of(cuts[0])
+        if causal:
+            column = lax.broadcasted_iota(jnp.int32, (chunk, chunk), 1)
+            line = lax.broadcasted_iota(jnp.int32, (chunk, chunk), 0)
             scores = jnp.where(column <= line, scores, -jnp.inf)
-        top = jnp.max(scores, axis=1, keepdims=True) + gate
-        weights = jnp.exp2(scores - (top - gate))
-        total = jnp.sum(weights, axis=1, keepdims=True)
-        held = weigh(weights, first)
-
-        def fold(source, state):
-            top, total, held = state
-            scores = scores_of(source)
-            newest = jnp.maximum(top, jnp.max(scores, axis=1, keepdims=True) + gate)
-            shrink = jnp.exp2(top - newest)
-            weights = jnp.exp2(scores - (newest - gate))
-            total = total * shrink + jnp.sum(weights, axis=1, keepdims=True)
-            held = held * shrink + weigh(weights, source)
-            return newest, total, held
-
-        top, total, held = lax.fori_loop(0, count, fold, (top, total, held))
-        return held / total, top + jnp.log(total) * LOG2E
+        top = jnp.max(scores, axis=1, keepdims=True)
+        held = None
+        for place, lines in enumerate(cuts):
+            later = scores_of(cuts[place + 1]) if place + 1 < len(cuts) else None
+            weights = jnp.exp2((scores - top) * factor).astype(jnp.bfloat16)
+            gained = jnp.dot(weights, v_buf[lines, :], preferred_element_type=jnp.float32)
+            held = gained if held is None else held + gained
+            if later is not None:
+                newest = jnp.maximum(top, jnp.max(later, axis=1, keepdims=True))
+                held = held * jnp.exp2((top - newest) * factor)
+                top, scores = newest, later
+        total = held[:, width:]
+        return held[:, :width] / total, top * factor + jnp.log(total) * LOG2E
 
     def back_copy(source, half):
         return to_ep(
             o_buf.at[source, half], attended.at[span(half, chunk), span(my_tp * heads + my_head, width)],
             send_o.at[source, half], recv_o.at[my_head, half], base + source,
         )
+
+    per_head = n // heads
 
     def give(source, half):
         @pl.when(source != my_head)
@@ -699,31 +765,24 @@
             ).start()
 
     def spread_step(step):
-        source = (me + n - step) % n
+        source = peer(step, -1)
         arrived(routed_piece(source)(my_tp), recv_a.at[source])
         spread(source)[0]()
 
-    per_head = n // heads
-
-    @pl.loop(0, heads)
-    def _(source):
-        for half in range(halves):
-            i = base + source
-            arrived(q_buf.at[i, half], recv_q.at[i, half])
-            out, lse = attend(i, half, source, source, True)
-
-            @pl.when(my_group == 0)
-            def _():
-                o_buf[source, half] = out.astype(o_buf.dtype)
-                give(source, half)
-
-            @pl.when(my_group > 0)
-            def _():
-                own_buf[source, half] = out
-                own_lse[source, half] = jnp.broadcast_to(lse, (chunk, width))
-
-        for s in range(per_head):
-            spread_step(source * per_head + s)
+    def own_queries(source, half):
+        i = base + source
+        arrived(q_spot(i, half), recv_q.at[i, half])
+        out, lse = attend(i, half, source * rows + (half + 1) * chunk, True)
+
+        @pl.when(my_group == 0)
+        def _():
+            o_buf[source, half] = out.astype(o_buf.dtype)
+            give(source, half)
+
+        @pl.when(my_group > 0)
+        def _():
+            own_buf[source, half] = out
+            own_lse[source, half] = lse
 
     def part_copies(i, half):
         slot = i % heads
@@ -736,25 +795,39 @@
                   (i // heads) * heads + my_head),
         )
 
-    def later_queries(half):
-        @pl.loop(base + heads, n)
-        def _(i):
-            arrived(q_buf.at[i, half], recv_q.at[i, half])
-            out, lse = attend(i, half, heads - 1, heads - 1, False)
+    def later_queries(group, source, half):
+        @pl.when(my_group + group < groups)
+        def _():
+            i = (my_group + group) * heads + source
+            arrived(q_spot(i, half), recv_q.at[i, half])
+            out, lse = attend(i, half, heads * rows, False)
             part_buf[i, half] = out.astype(part_buf.dtype)
-            part_lse[i, half] = jnp.broadcast_to(lse, (chunk, width)).T[: part_lse.shape[2], :]
+            part_lse[i, half] = lse.T[: part_lse.shape[2], :]
             for copy in part_copies(i, half):
                 copy.start()
 
-    later_queries(0)
+    def later_all(half):
+        for group in range(1, groups):
+            @pl.loop(0, heads)
+            def _(source):
+                later_queries(group, source, half)
+
+    for step in range(n):
+        spread_step(step)
+        if step >= 2:
+            spread(peer(step - 2, -1))[1]()
+        if step < heads:
+            own_queries(step, 0)
+        elif step < 2 * heads:
+            for group in range(1, groups):
+                later_queries(group, step - heads, 0)
+
+    for step in range(n - 2, n):
+        spread(peer(step, -1))[1]()
 
     @pl.loop(0, n)
-    def _(step):
-        spread((me + n - step) % n)[1]()
-
-    @pl.loop(0, n)
-    def _(step):
-        spread((me + n - step) % n)[2]()
+    def _(source):
+        spread(source)[2]()
 
     loads[1].wait()
     loads[2].wait()
@@ -767,7 +840,25 @@
         ).astype(hidden.dtype)
         hidden_gather(part)[0]()
 
-    later_queries(1)
+    def give_mixed(half):
+        @pl.loop(0, heads)
+        def _(step):
+            head = (my_head + step) % heads
+            arrived(
+                attended.at[span(half, chunk), span(my_tp * heads + head, width)],
+                recv_o.at[head, half],
+            )
+        mixed_gather(half)[0]()
+
+    for half in range(1, halves):
+        for source in range(heads):
+            own_queries(source, half)
+        later_all(half)
+
+    @pl.when(my_group == 0)
+    def _():
+        for half in range(halves):
+            give_mixed(half)
 
     for part in range(parts):
         hidden_gather(part)[1]()
@@ -799,79 +890,90 @@
 
     merge(0)
 
+    def mix(half):
+        mixed_gather(half)[1]()
+        mixed_gather(half)[2]()
+        lines = span(half, chunk)
+        mixed_ref[lines, :] = jnp.dot(
+            attended[lines, :], wo[...], preferred_element_type=jnp.float32
+        ).astype(mixed_ref.dtype)
+
     for part in range(parts):
         hidden_gather(part)[2]()
     loads[3].wait()
-    tiles = 2
-    tall = n * capacity // tiles
-    each = n // tiles
-
-    def return_copy(target):
+    tall = heads * capacity
+
+    def return_copy(group, head):
+        source = group * heads + head
         return to_ep(
-            product.at[span(target, capacity), :], back.at[span(me, capacity), :],
-            send_r.at[target], recv_r.at[me], target,
-        )
-
-    @pl.loop(0, tiles)
-    def _(step):
-        tile = (step + 1 + me // each) % tiles
-        lines = span(tile, tall)
+            product.at[span(source, capacity), :],
+            back.at[span(group * heads + my_head, capacity), :],
+            send_r.at[source], recv_r.at[group * heads + my_head], base + head,
+        )
+
+    def down(group):
+        lines = span(group, tall)
         product[lines, :] = jnp.dot(
             hidden[lines, :], wd[...], preferred_element_type=jnp.float32
         ).astype(product.dtype)
 
-        @pl.loop(0, each)
-        def _(place):
-            target = tile * each + (place + me) % each
-
-            @pl.when(target != me)
-            def _():
-                return_copy(target).start()
-
-            @pl.when(target == me)
-            def _():
-                pltpu.make_async_copy(
-                    product.at[span(me, capacity), :], back.at[span(me, capacity), :], recv_r.at[me]
-                ).start()
+    def hand_back(group):
+        mine = span(group * heads + my_head, capacity)
+        pltpu.make_async_copy(
+            product.at[mine, :], back.at[mine, :], recv_r.at[group * heads + my_head]
+        ).start()
+        for step in range(1, heads):
+            return_copy(group, (my_head + step) % heads).start()
+
+    def combined(group):
+        for step in range(heads):
+            place = group * heads + (my_head + step) % heads
+            arrived(back.at[span(place, capacity), :], recv_r.at[place])
+        lines = span(group, tall)
+        return jnp.dot(
+            comb_hi[group], back[lines, :], preferred_element_type=jnp.float32
+        ) + jnp.dot(comb_lo[group], back[lines, :], preferred_element_type=jnp.float32)
+
+    def sum_copy(group):
+        return to_ep(
+            sums_out.at[group], sums_in.at[my_group], send_c.at[group], recv_c.at[my_group],
+            group * heads + my_head,
+        )
+
+    for group in others:
+        down(group)
+        hand_back(group)
+    down(my_group)
 
     for half in range(1, halves):
         merge(half)
 
-    @pl.loop(0, heads)
-    def _(step):
-        head = (my_head + step) % heads
-        for half in range(halves):
-            arrived(
-                attended.at[span(half, chunk), span(my_tp * heads + head, width)],
-                recv_o.at[head, half],
-            )
-        mixed_gather(head)[0]()
-
-    @pl.loop(0, heads)
-    def _(step):
-        mixed_gather((my_head + step) % heads)[1]()
-
-    @pl.loop(0, heads)
-    def _(head):
-        mixed_gather(head)[2]()
+    @pl.when(my_group > 0)
+    def _():
+        give_mixed(0)
+
+
+    for group in others:
+        sums_out[group] = combined(group).astype(sums_out.dtype)
+        sum_copy(group).start()
+
+    hand_back(my_group)
+
+    @pl.when(my_group > 0)
+    def _():
+        for half in range(1, halves):
+            give_mixed(half)
+
 
     loads[4].wait()
-
-    @pl.loop(0, 2)
-    def _(step):
-        lines = span(step, rows // 2)
-        mixed_ref[lines, :] = jnp.dot(
-            attended[lines, :], wo[...], preferred_element_type=jnp.float32
-        ).astype(mixed_ref.dtype)
-
-    @pl.loop(0, n)
-    def _(source):
-        arrived(back.at[span(source, capacity), :], recv_r.at[source])
-
-    expert_ref[...] = (
-        jnp.dot(comb_hi[...], back[...], preferred_element_type=jnp.float32)
-        + jnp.dot(comb_lo[...], back[...], preferred_element_type=jnp.float32)
-    ).astype(expert_ref.dtype)
+    for half in range(halves):
+        mix(half)
+
+    expert_sum = combined(my_group)
+    for group in others:
+        arrived(sums_in.at[group], recv_c.at[group])
+        expert_sum = expert_sum + sums_in[group].astype(jnp.float32)
+    expert_ref[...] = expert_sum.astype(expert_ref.dtype)
 
     token_gather[3]()
 
@@ -900,7 +1002,14 @@
     @pl.loop(1, n)
     def _(step):
         leave_copy((me + step) % n).wait_send()
-        return_copy((me + step) % n).wait_send()
+
+    for group in [my_group, *others]:
+        for step in range(1, heads):
+            return_copy(group, (my_head + step) % heads).wait_send()
+    for group in others:
+        sum_copy(group).wait_send()
+        for copy in route_copies(group):
+            copy.wait_send()
 
     @pl.loop(0, n)
     def _(source):
@@ -909,9 +1018,8 @@
     for part in range(parts):
         hidden_gather(part)[3]()
 
-    @pl.loop(0, heads)
-    def _(head):
-        mixed_gather(head)[3]()
+    for half in range(halves):
+        mixed_gather(half)[3]()
 
 
 def fused(
@@ -949,9 +1057,15 @@
             pltpu.VMEM((n * share, depth), half_type), pltpu.VMEM((slots, depth), half_type),
             pltpu.VMEM((slots, inner * tp), half_type), pltpu.VMEM((slots, out_width), half_type),
             pltpu.VMEM((slots, out_width), half_type),
-            pltpu.VMEM((block_rows, slots), half_type), pltpu.VMEM((block_rows, slots), half_type),
-            pltpu.VMEM((heads, rows, width), half_type), pltpu.VMEM((heads, rows, width), half_type),
-            pltpu.VMEM((n, halves, chunk, width), half_type),
+            pltpu.VMEM((groups, block_rows, heads * capacity), half_type),
+            pltpu.VMEM((groups, block_rows, heads * capacity), half_type),
+            pltpu.VMEM((groups, chosen, block_rows), jnp.int32),
+            pltpu.VMEM((groups, chosen, block_rows), wide),
+            pltpu.VMEM((groups, block_rows, out_width), half_type),
+            pltpu.VMEM((groups, block_rows, out_width), half_type),
+            pltpu.VMEM((heads * rows, 2 * width), half_type),
+            pltpu.VMEM((heads * rows, 2 * width), half_type),
+            pltpu.VMEM((n, halves, chunk, 2 * width), half_type),
             pltpu.VMEM((heads, halves, chunk, width), half_type),
             pltpu.VMEM((heads, halves, chunk, width), wide),
             pltpu.VMEM((heads, halves, chunk, width), wide),
@@ -966,7 +1080,8 @@
             dma((n, halves)), dma((groups, heads * halves)),
             dma((tp, tp)), dma((tp,)), dma((n,)), dma((n,)), dma((n * tp, tp)), dma((n * tp,)),
             dma((parts * tp, tp)), dma((parts * tp,)), dma((n,)), dma((n,)),
-            dma((heads * tp, tp)), dma((heads * tp,)),
+            dma((halves * tp, tp)), dma((halves * tp,)),
+            dma((groups,)), dma((groups,)), dma((groups,)), dma((groups,)), dma((groups,)), dma((groups,)),
         ],
         compiler_params=pltpu.CompilerParams(
             collective_id=0, has_side_effects=True, vmem_limit_bytes=58 * 1024 * 1024
@@ -1028,5 +1143,6 @@
         P("ep", None, "tp"),
     )
     return jax.shard_map(
-        functools.partial(choose, chip_cores(mesh)), mesh=mesh, in_specs=placed, out_specs=(P("ep", "tp"), P("ep", "tp")), check_vma=False
+        functools.partial(choose, chip_cores(mesh)), mesh=mesh, in_specs=placed,
+        out_specs=(P("ep", "tp"), P("ep", "tp")), check_vma=False,
     )

time: 126 us -> 106 us (0.84)
  Pallas kernels: 121 us -> 101 us
    pallas_call x1, Pallas kernels: 121 us -> 101 us  [fused(): pl.pallas_call(functools.partial(fused_kernel, n, tp, heads, cores), out_...]
where the time goes in v2:
time: 106 us
  Pallas kernels  101 us (95%)
  local copies, waits for them, and re-layouts  3.93 us (4%)
    pallas_call x1, Pallas kernels, fused(): pl.pallas_call(functools.partial(fused_kernel, n, tp, heads, cores), out_...  101 us
    unnamed x2, local copies, waits for them, and re-layouts  3.93 us

profile of v2, /device:TPU:27, one launch (start us, length us, event | category | flops | bytes accessed | tf_op | source)
XLA Modules:
  0.0 105.8 jit_solution(3322438011800505623)
XLA Ops:
  0.6 101.2 %shard_map.131 = (bf16[512,1024]{1,0:T(8,128)(2,1)}, bf16[128,1024]{1,0:T(8,128)(2,1)}) custom-call(bf16[512,512]{1,0:T(8,128)(2,1)} %q_ref.1, bf16[512,512]{1,0:T(8,128)(2,1)} %k_ref.1, bf16[512,512]{1,0:T(8,128)(2,1)} %v_ref.1, f32[4,4096]{1,0:T(4,128)} %bitcast.4, bf16[32,4096]{1,0:T(8,128)(2,1)} %x_ref.1, f32[1,4096]{1,0:T(1,128)} %bitcast.5, ...), custom_call_target="tpu_custom_call" | custom-call | flops 8589934592 | bytes 16777216 | tf_op jit(solution)/shard_map/pallas_call | solution.py:1044
  101.9 2.3 %copy.16 = bf16[512,1024]{1,0:T(8,128)(2,1)} copy(bf16[512,1024]{1,0:T(8,128)(2,1)} %get-tuple-element.4) | data formatting | bytes 2097152
  104.1 1.7 %copy.17 = bf16[128,1024]{1,0:T(8,128)(2,1)} copy(bf16[128,1024]{1,0:T(8,128)(2,1)} %get-tuple-element.5) | data formatting | bytes 524288

commit v3 on v2

--- a/solution.py
+++ b/solution.py
@@ -491,7 +491,8 @@
     def mixed_gather(half):
         return gather(mixed_piece(half), send_m, recv_m, half * tp)
 
-    across_groups = [(g, (heads // 2 + s) % heads) for g in range(1, groups) for s in range(heads)]
+    straight = [(heads // 2 + s) % heads for s in (*range(0, heads, 2), *range(1, heads, 2))]
+    across_groups = [(g, s) for g in range(1, groups) for s in straight]
     in_group = [(0, s) for s in range(1, heads)]
     order = [(0, 0)]
     for place in range(max(len(across_groups), len(in_group))):

time: 106 us -> 104 us (0.981)
  Pallas kernels: 101 us -> 99.3 us
    pallas_call x1, Pallas kernels: 101 us -> 99.3 us  [fused(): pl.pallas_call(functools.partial(fused_kernel, n, tp, heads, cores), out_...]
where the time goes in v3:
time: 104 us
  Pallas kernels  99.3 us (95%)
  local copies, waits for them, and re-layouts  3.93 us (4%)
    pallas_call x1, Pallas kernels, fused(): pl.pallas_call(functools.partial(fused_kernel, n, tp, heads, cores), out_...  99.3 us
    unnamed x2, local copies, waits for them, and re-layouts  3.93 us

profile of v3, /device:TPU:27, one launch (start us, length us, event | category | flops | bytes accessed | tf_op | source)
XLA Modules:
  0.0 103.9 jit_solution(17639397984493551341)
XLA Ops:
  0.6 99.3 %shard_map.131 = (bf16[512,1024]{1,0:T(8,128)(2,1)}, bf16[128,1024]{1,0:T(8,128)(2,1)}) custom-call(bf16[512,512]{1,0:T(8,128)(2,1)} %q_ref.1, bf16[512,512]{1,0:T(8,128)(2,1)} %k_ref.1, bf16[512,512]{1,0:T(8,128)(2,1)} %v_ref.1, f32[4,4096]{1,0:T(4,128)} %bitcast.4, bf16[32,4096]{1,0:T(8,128)(2,1)} %x_ref.1, f32[1,4096]{1,0:T(1,128)} %bitcast.5, ...), custom_call_target="tpu_custom_call" | custom-call | flops 8589934592 | bytes 16777216 | tf_op jit(solution)/shard_map/pallas_call | solution.py:1045
  100.0 2.3 %copy.16 = bf16[512,1024]{1,0:T(8,128)(2,1)} copy(bf16[512,1024]{1,0:T(8,128)(2,1)} %get-tuple-element.4) | data formatting | bytes 2097152
  102.2 1.7 %copy.17 = bf16[128,1024]{1,0:T(8,128)(2,1)} copy(bf16[128,1024]{1,0:T(8,128)(2,1)} %get-tuple-element.5) | data formatting | bytes 524288
